TPU v7x, 32 devices: a whole 2x2x4 slice. The times are simulated.
32 devices in a mesh: fs: 8 (over z, core), tp: 4 (over y, x).
Axes of the slice: x: 2, y: 2, z: 4, core: 2. Of those that a mesh axis runs over, the one named last changes fastest.
Arguments:
- normed_in: bfloat16 [8192, 2048], P('fs'), may hold values from -6 to 6
- grad_x: bfloat16 [8192, 2048], P('fs', 'tp'), may hold values from -0.088388348 to 0.088388348
- grad_y: bfloat16 [8192, 2048], P('fs', 'tp'), may hold values from -0.088388348 to 0.088388348
- weight_x: float32 [2048, 2048], P('fs', 'tp'), may hold values from -0.125 to 0.125
- weight_y: float32 [2048, 2048], P('fs', 'tp'), may hold values from -0.125 to 0.125
- factor_x: bfloat16 [2048, 512], P('fs'), may hold values from -0.13258252 to 0.13258252
- factor_y: bfloat16 [2048, 512], P('fs'), may hold values from -0.13258252 to 0.13258252
- first_x: float32 [512, 2048], P('fs', 'tp'), may hold values from -8 to 8
- first_y: float32 [512, 2048], P('fs', 'tp'), may hold values from -8 to 8
- second_x: float32 [512, 2048], P('fs', 'tp'), may hold values from 0.5 to 2
- second_y: float32 [512, 2048], P('fs', 'tp'), may hold values from 0.5 to 2
Outputs:
- new_weight_x: float32 [2048, 2048], P('fs', 'tp')
- new_weight_y: float32 [2048, 2048], P('fs', 'tp')
- step_x: float32 [2048, 2048], P('fs', 'tp')
- step_y: float32 [2048, 2048], P('fs', 'tp')
- new_first_x: float32 [512, 2048], P('fs', 'tp')
- new_first_y: float32 [512, 2048], P('fs', 'tp')
- new_second_x: float32 [512, 2048], P('fs', 'tp')
- new_second_y: float32 [512, 2048], P('fs', 'tp')
- copy_x: bfloat16 [2048, 2048], P(None, 'tp')
- copy_y: bfloat16 [2048, 2048], P(None, 'tp')
All inputs are finite; a program needn't handle non-finite values.
Results may differ from a plain program's by a relative error of at most 0.02.
Values may be sent and summed in bfloat16 or wider, within the bound.
A program may use at most 128 MiB of HBM per device.

v0:
```python
import jax
import jax.numpy as jnp
from jax import lax
from jax.sharding import PartitionSpec as P

D = 2048
RW = 2048


def on_device(
    normed_in,
    grad_x,
    grad_y,
    weight_x,
    weight_y,
    factor_x,
    factor_y,
    first_x,
    first_y,
    second_x,
    second_y,
):
    width = grad_x.shape[1]
    contract = (((0,), (0,)), ((), ()))
    highest = lax.Precision.HIGHEST
    cotangent = jnp.concatenate((grad_x, grad_y), 1)
    summed = lax.psum_scatter(
        lax.dot_general(normed_in, cotangent, contract, preferred_element_type=jnp.float32).astype(
            jnp.bfloat16
        ),
        "fs",
        scatter_dimension=0,
        tiled=True,
    ).astype(jnp.float32)
    part_x = factor_x.astype(jnp.float32)
    part_y = factor_y.astype(jnp.float32)
    low_x = lax.dot_general(part_x, summed[:, :width], contract, precision=highest)
    low_y = lax.dot_general(part_y, summed[:, width:], contract, precision=highest)
    projected = lax.psum_scatter(
        jnp.concatenate((low_x, low_y), 1), "fs", scatter_dimension=0, tiled=True
    )
    low_x = projected[:, :width]
    low_y = projected[:, width:]
    new_first_x = 0.8 * first_x + 0.2 * low_x
    new_first_y = 0.8 * first_y + 0.2 * low_y
    new_second_x = 0.9 * second_x + 0.1 * low_x * low_x
    new_second_y = 0.9 * second_y + 0.1 * low_y * low_y
    direction = jnp.concatenate(
        (new_first_x / jnp.sqrt(new_second_x), new_first_y / jnp.sqrt(new_second_y)), 1
    )
    piece = lax.all_gather(direction, "fs", axis=0, tiled=True)
    part_x = factor_x.astype(jnp.float32)
    part_y = factor_y.astype(jnp.float32)
    update_x = jnp.dot(part_x, piece[:, :width], precision=highest)
    update_y = jnp.dot(part_y, piece[:, width:], precision=highest)
    total = lax.psum(jnp.sum(update_x * update_x) + jnp.sum(update_y * update_y), ("fs", "tp"))
    scale = jnp.minimum(1.0, 0.25 * jnp.sqrt(2.0 * D * RW) / jnp.sqrt(total))
    step_x = scale * update_x
    step_y = scale * update_y
    new_x = weight_x - 0.02 * step_x
    new_y = weight_y - 0.02 * step_y
    copy_x, copy_y = (
        lax.all_gather(new_x.astype(jnp.bfloat16), "fs", axis=0, tiled=True),
        lax.all_gather(new_y.astype(jnp.bfloat16), "fs", axis=0, tiled=True),
    )
    return (
        new_x,
        new_y,
        step_x,
        step_y,
        new_first_x,
        new_first_y,
        new_second_x,
        new_second_y,
        copy_x,
        copy_y,
    )


def solution(mesh):
    in_specs = (
        P("fs", None),
        P("fs", "tp"),
        P("fs", "tp"),
        P("fs", "tp"),
        P("fs", "tp"),
        P("fs", None),
        P("fs", None),
        P("fs", "tp"),
        P("fs", "tp"),
        P("fs", "tp"),
        P("fs", "tp"),
    )
    out_specs = (
        P("fs", "tp"),
        P("fs", "tp"),
        P("fs", "tp"),
        P("fs", "tp"),
        P("fs", "tp"),
        P("fs", "tp"),
        P("fs", "tp"),
        P("fs", "tp"),
        P(None, "tp"),
        P(None, "tp"),
    )
    return jax.shard_map(
        on_device, mesh=mesh, in_specs=in_specs, out_specs=out_specs, check_vma=False
    )
```

profile of v0, /device:TPU:9, one launch (start us, length us, event | category | flops | bytes accessed | tf_op | source)
XLA Modules:
  0.0 260.7 jit_solution(1484371934440592451)
XLA Ops:
  7.2 0.0 reduce-scatter.5.cloned.1.call-start
  7.2 9.4 %convert_bitcast_fusion = bf16[2048,1024]{0,1:T(8,128)(2,1)} fusion(bf16[1024,2048]{1,0:T(8,128)(2,1)} %param.11, bf16[1024,512]{1,0:T(8,128)(2,1)} %param.13, bf16[1024,512]{1,0:T(8,128)(2,1)} %param.12), kind=kOutput, calls=%fused_computation | convolution fusion | flops 4301258752 | bytes 10485760 | tf_op jit(solution)/shard_map/dot_general | solution.py:28
  16.6 0.0 reduce-scatter.5.cloned.1.call-update
  16.6 0.0 reduce-scatter.7.cloned.1.call-start
  16.7 50.0 %reduce-scatter.5.cloned.1.call-done = bf16[256,1024]{0,1:T(8,128)(2,1)} async-done(((bf16[2048,1024]{0,1:T(8,128)(2,1)}), bf16[256,1024]{0,1:T(8,128)(2,1)}) %reduce-scatter.5.cloned.1.call-update) | async-done | bytes 524304 | tf_op jit(solution)/shard_map/reduce_scatter | solution.py:27
  66.7 1.2 convolution_bitcast_fusion
  67.9 1.2 convolution_bitcast_fusion.1
  69.1 0.2 pad_maximum_fusion
  69.3 1.8 copy.64
  71.1 0.0 reduce-scatter.7.cloned.1.call-update
  71.2 0.0 all-gather.4.cloned.1.call-start
  71.2 30.5 %reduce-scatter.7.cloned.1.call-done = f32[64,1024]{1,0:T(8,128)} async-done(((f32[512,1024]{1,0:T(8,128)}), f32[64,1024]{1,0:T(8,128)}) %reduce-scatter.7.cloned.1.call-update) | async-done | bytes 262160 | tf_op jit(solution)/shard_map/reduce_scatter | solution.py:39
  101.8 1.8 rsqrt_multiply_fusion.1
  103.6 0.7 pad_maximum_fusion.1
  104.3 0.0 all-gather.8.cloned.1.call-start
  104.4 33.4 %all-gather.4.cloned.1.call-done = f32[512,1024]{1,0:T(8,128)} async-done(((f32[64,1024]{1,0:T(8,128)}), f32[512,1024]{1,0:T(8,128)}) %all-gather.4.cloned.1.call-update) | async-done | bytes 2097168 | tf_op jit(solution)/shard_map/all_gather | solution.py:51
  137.8 2.8 %multiply_reduce_fusion = (f32[]{:T(128)}, f32[512,256]{1,0:T(8,128)S(1)}) fusion(bf16[256,512]{1,0:T(8,128)(2,1)S(1)} %copy-done, f32[512,1024]{1,0:T(8,128)} %all-gather.4.cloned.1.call-done), kind=kOutput, calls=%fused_computation.15 | convolution fusion | flops 805568512 | bytes 1835012 | tf_op jit(solution)/shard_map/dot_general | solution.py:55
  140.6 2.8 %multiply_reduce_fusion.1 = (f32[]{:T(128)}, f32[512,256]{1,0:T(8,128)S(1)}) fusion(bf16[256,512]{1,0:T(8,128)(2,1)S(1)} %copy-done.1, f32[512,1024]{1,0:T(8,128)} %all-gather.4.cloned.1.call-done), kind=kOutput, calls=%fused_computation.16 | convolution fusion | flops 805568512 | bytes 1835012 | tf_op jit(solution)/shard_map/dot_general | solution.py:54
  144.8 0.2 copy.57
  145.0 38.1 %psum.7 = f32[]{:T(128)} all-reduce(f32[]{:T(128)S(6)} %add.25), channel_id=1, replica_groups=mesh['fs'=8,'tp'=4] {'fs','tp'}, use_global_device_ids=true, to_apply=%region_4.0 | all-reduce | flops 1 | bytes 8 | tf_op jit(solution)/shard_map/psum | solution.py:56
  183.8 0.8 fusion.12
  184.6 0.0 all-gather.6.cloned.1.call-start
  184.7 1.2 copy.56
  185.9 0.8 fusion.13
  186.8 1.0 copy.58
  187.7 1.0 copy.60
  188.7 1.0 copy.59
  189.7 1.0 copy.61
  190.7 27.9 %all-gather.8.cloned.1.call-done = bf16[2048,512]{0,1:T(8,128)(2,1)} async-done(((bf16[256,512]{0,1:T(8,128)(2,1)}), bf16[2048,512]{0,1:T(8,128)(2,1)}) %all-gather.8.cloned.1.call-update) | async-done | bytes 2097168 | tf_op jit(solution)/shard_map/all_gather | solution.py:64
  218.6 3.9 %copy.63 = bf16[2048,512]{1,0:T(8,128)(2,1)} copy(bf16[2048,512]{0,1:T(8,128)(2,1)} %all-gather.8.cloned.1.call-done) | data formatting | bytes 4194304
  222.5 27.8 %all-gather.6.cloned.1.call-done = bf16[2048,512]{0,1:T(8,128)(2,1)} async-done(((bf16[256,512]{0,1:T(8,128)(2,1)}), bf16[2048,512]{0,1:T(8,128)(2,1)}) %all-gather.6.cloned.1.call-update) | async-done | bytes 2097168 | tf_op jit(solution)/shard_map/all_gather | solution.py:63
  250.3 3.9 %copy.62 = bf16[2048,512]{1,0:T(8,128)(2,1)} copy(bf16[2048,512]{0,1:T(8,128)(2,1)} %all-gather.6.cloned.1.call-done) | data formatting | bytes 4194304
  (17 shorter events, 0.1 us)
Async XLA Ops:
  7.2 59.5 %copy-start = (bf16[256,512]{1,0:T(8,128)(2,1)S(1)}, bf16[256,512]{1,0:T(8,128)(2,1)}, u32[]{:S(2)}) copy-start(bf16[256,512]{1,0:T(8,128)(2,1)} %param.17) | copy-start | bytes 786436
  7.2 59.5 %reduce-scatter.5.cloned.1.call-start = ((), (), s32[]{:S(2)}) async-start(), calls=%async_computation.2 | async-start | bytes 4718592 | tf_op jit(solution)/shard_map/reduce_scatter | solution.py:27
  16.6 51.3 %copy-start.1 = (bf16[256,512]{1,0:T(8,128)(2,1)S(1)}, bf16[256,512]{1,0:T(8,128)(2,1)}, u32[]{:S(2)}) copy-start(bf16[256,512]{1,0:T(8,128)(2,1)} %param.16) | copy-start | bytes 786436
  16.6 85.1 %reduce-scatter.7.cloned.1.call-start = ((), (), s32[]{:S(2)}) async-start(), calls=%async_computation.6 | async-start | bytes 2359296 | tf_op jit(solution)/shard_map/reduce_scatter | solution.py:39
  71.1 30.6 %copy-start.3 = (f32[64,512]{1,0:T(8,128)S(1)}, f32[64,512]{1,0:T(8,128)}, u32[]{:S(2)}) copy-start(f32[64,512]{1,0:T(8,128)} %param.20) | copy-start | bytes 393220
  71.1 30.6 %copy-start.4 = (f32[64,512]{1,0:T(8,128)S(1)}, f32[64,512]{1,0:T(8,128)}, u32[]{:S(2)}) copy-start(f32[64,512]{1,0:T(8,128)} %param.18) | copy-start | bytes 393220
  71.1 30.6 %copy-start.5 = (f32[64,512]{1,0:T(8,128)S(1)}, f32[64,512]{1,0:T(8,128)}, u32[]{:S(2)}) copy-start(f32[64,512]{1,0:T(8,128)} %param.21) | copy-start | bytes 393220
  71.1 30.6 %copy-start.6 = (f32[64,512]{1,0:T(8,128)S(1)}, f32[64,512]{1,0:T(8,128)}, u32[]{:S(2)}) copy-start(f32[64,512]{1,0:T(8,128)} %param.19) | copy-start | bytes 393220
  71.2 66.6 %all-gather.4.cloned.1.call-start = ((), (), s32[]{:S(2)}) async-start(), calls=%async_computation.3 | async-start | bytes 2359296 | tf_op jit(solution)/shard_map/all_gather | solution.py:51
  104.3 40.5 %copy-start.2 = (f32[256,512]{1,0:T(8,128)S(1)}, f32[256,512]{1,0:T(8,128)}, u32[]{:S(2)}) copy-start(f32[256,512]{1,0:T(8,128)} %param.15) | copy-start | bytes 1572868
  104.3 114.3 %all-gather.8.cloned.1.call-start = ((), (), s32[]{:S(2)}) async-start(), calls=%async_computation.5 | async-start | bytes 2359296 | tf_op jit(solution)/shard_map/all_gather | solution.py:64
  184.6 65.7 %all-gather.6.cloned.1.call-start = ((), (), s32[]{:S(2)}) async-start(), calls=%async_computation.4 | async-start | bytes 2359296 | tf_op jit(solution)/shard_map/all_gather | solution.py:63
Sparse Core Ops, SparseCore 0:
  16.8 49.8 reduce-scatter.4
  71.3 30.4 reduce-scatter.6
  104.5 33.2 all-gather.3
  184.7 33.8 all-gather.7
  220.6 29.6 all-gather.5
where the time goes:
time: 261 us
  waiting for transfers between devices  170 us (65%)
  blocking collectives  38.1 us (15%)
  matrix products  17.5 us (7%)
  between operations  15.9 us (6%)
  local copies, waits for them, and re-layouts  15.1 us (6%)
  other arithmetic  4.31 us (2%)
    reduce_scatter x1, waiting for transfers between devices, on_device(): lax.psum_scatter(lax.dot_general(normed_in, cotangent, contract, preferre...  50 us
    psum x1, blocking collectives, on_device(): lax.psum(jnp.sum(update_x * update_x) + jnp.sum(update_y * update_y), ('f...  38.1 us
    all_gather x1, waiting for transfers between devices, on_device(): piece = lax.all_gather(direction, 'fs', axis=0, tiled=True)  33.4 us
    reduce_scatter x1, waiting for transfers between devices, on_device(): lax.psum_scatter(jnp.concatenate((low_x, low_y), 1), 'fs', scatter_dimens...  30.5 us
    all_gather x1, waiting for transfers between devices, on_device(): lax.all_gather(new_y.astype(jnp.bfloat16), 'fs', axis=0, tiled=True)  27.9 us
    all_gather x1, waiting for transfers between devices, on_device(): lax.all_gather(new_x.astype(jnp.bfloat16), 'fs', axis=0, tiled=True)  27.8 us
    unnamed x23, local copies, waits for them, and re-layouts  15.1 us
    dot_general x1, matrix products, on_device(): lax.dot_general(normed_in, cotangent, contract, preferred_element_type=jn...  9.38 us
  transfers between devices with their start and end apart: 5, of which 5 were waited for; matrix products, arithmetic and copies ran while one was open for 4% of the time, Pallas kernels for 0%

commit v1 on v0

--- a/solution.py
+++ b/solution.py
@@ -48,7 +48,12 @@
     direction = jnp.concatenate(
         (new_first_x / jnp.sqrt(new_second_x), new_first_y / jnp.sqrt(new_second_y)), 1
     )
-    piece = lax.all_gather(direction, "fs", axis=0, tiled=True)
+    ring = [direction]
+    for hop in range(7):
+        ring.append(lax.ppermute(ring[-1], "fs", [(dev, (dev + 1) % 8) for dev in range(8)]))
+    piece = jnp.roll(
+        jnp.concatenate(ring[::-1], axis=0), (lax.axis_index("fs") + 1) * ring[0].shape[0], axis=0
+    )
     part_x = factor_x.astype(jnp.float32)
     part_y = factor_y.astype(jnp.float32)
     update_x = jnp.dot(part_x, piece[:, :width], precision=highest)

time: 261 us -> 284 us (1.088)
  blocking collectives: 38.1 us -> 54 us
  starting transfers between devices: 0.21 us -> 13.3 us
  waiting for transfers between devices: 170 us -> 165 us
    all_gather x1 -> x0, waiting for transfers between devices: 33.4 us -> none  [on_device(): piece = lax.all_gather(direction, 'fs', axis=0, tiled=True)]
    ppermute x0 -> x7, waiting for transfers between devices: none -> 30.1 us  [on_device(): lax.ppermute(ring[-1], 'fs', [(dev, (dev + 1) % 8) for dev in range(8)])]
    psum x1, blocking collectives: 38.1 us -> 54 us  [on_device(): lax.psum(jnp.sum(update_x * update_x) + jnp.sum(update_y * update_y), ('f...]
    ppermute x0 -> x7, starting transfers between devices: none -> 13.2 us  [on_device(): lax.ppermute(ring[-1], 'fs', [(dev, (dev + 1) % 8) for dev in range(8)])]
    unnamed x23 -> x35, local copies, waits for them, and re-layouts: 15.1 us -> 16.4 us
  transfers between devices with their start and end apart: 5 -> 11, of which waited for: 5 -> 11; matrix products, arithmetic and copies ran while one was open for 4% -> 4% of each run, Pallas kernels for 0% -> 0%
where the time goes in v1:
time: 284 us; the launch traced here: 283 us
  waiting for transfers between devices  165 us (58%)
  blocking collectives  54 us (19%)
  local copies, waits for them, and re-layouts  16.4 us (6%)
  between operations  16 us (6%)
  matrix products  15.1 us (5%)
  starting transfers between devices  13.3 us (5%)
  other arithmetic  3.66 us (1%)
    psum x1, blocking collectives, on_device(): lax.psum(jnp.sum(update_x * update_x) + jnp.sum(update_y * update_y), ('f...  54 us
    reduce_scatter x1, waiting for transfers between devices, on_device(): lax.psum_scatter(lax.dot_general(normed_in, cotangent, contract, preferre...  50 us
    reduce_scatter x1, waiting for transfers between devices, on_device(): lax.psum_scatter(jnp.concatenate((low_x, low_y), 1), 'fs', scatter_dimens...  30.3 us
    ppermute x7, waiting for transfers between devices, on_device(): lax.ppermute(ring[-1], 'fs', [(dev, (dev + 1) % 8) for dev in range(8)])  30.1 us
    all_gather x1, waiting for transfers between devices, on_device(): lax.all_gather(new_x.astype(jnp.bfloat16), 'fs', axis=0, tiled=True)  27.8 us
    all_gather x1, waiting for transfers between devices, on_device(): lax.all_gather(new_y.astype(jnp.bfloat16), 'fs', axis=0, tiled=True)  26.7 us
    unnamed x35, local copies, waits for them, and re-layouts  16.4 us
    ppermute x7, starting transfers between devices, on_device(): lax.ppermute(ring[-1], 'fs', [(dev, (dev + 1) % 8) for dev in range(8)])  13.2 us
  transfers between devices with their start and end apart: 11, of which 11 were waited for; matrix products, arithmetic and copies ran while one was open for 4% of the time, Pallas kernels for 0%

profile of v1, /device:TPU:9, one launch (start us, length us, event | category | flops | bytes accessed | tf_op | source)
XLA Modules:
  0.0 283.4 jit_solution(18360407224039292054)
XLA Ops:
  7.2 9.4 %convert_bitcast_fusion = bf16[2048,1024]{0,1:T(8,128)(2,1)} fusion(bf16[1024,2048]{1,0:T(8,128)(2,1)} %param.11, bf16[1024,512]{1,0:T(8,128)(2,1)} %param.13, bf16[1024,512]{1,0:T(8,128)(2,1)} %param.12), kind=kOutput, calls=%fused_computation | convolution fusion | flops 4301258752 | bytes 10485760 | tf_op jit(solution)/shard_map/dot_general | solution.py:28
  16.7 50.0 %reduce-scatter.5.cloned.1.call-done = bf16[256,1024]{0,1:T(8,128)(2,1)} async-done(((bf16[2048,1024]{0,1:T(8,128)(2,1)}), bf16[256,1024]{0,1:T(8,128)(2,1)}) %reduce-scatter.5.cloned.1.call-update) | async-done | bytes 524304 | tf_op jit(solution)/shard_map/reduce_scatter | solution.py:27
  66.7 1.2 convolution_bitcast_fusion
  67.9 1.2 convolution_bitcast_fusion.1
  69.4 1.8 copy.63
  71.3 30.3 %reduce-scatter.7.cloned.1.call-done = f32[64,1024]{1,0:T(8,128)} async-done(((f32[512,1024]{1,0:T(8,128)}), f32[64,1024]{1,0:T(8,128)}) %reduce-scatter.7.cloned.1.call-update) | async-done | bytes 262160 | tf_op jit(solution)/shard_map/reduce_scatter | solution.py:39
  101.6 1.8 rsqrt_multiply_fusion.1
  103.4 1.1 collective-permute-start
  104.6 3.3 %collective-permute-done = f32[64,1024]{1,0:T(8,128)S(1)} collective-permute-done((f32[64,1024]{1,0:T(8,128)S(1)}, f32[64,1024]{1,0:T(8,128)S(1)}, u32[]{:S(2)}, u32[]{:S(2)}) %collective-permute-start) | collective-permute-done | bytes 262176 | tf_op jit(solution)/shard_map/ppermute | solution.py:53
  107.9 2.5 collective-permute-start.1
  110.4 3.3 %collective-permute-done.1 = f32[64,1024]{1,0:T(8,128)S(1)} collective-permute-done((f32[64,1024]{1,0:T(8,128)S(1)}, f32[64,1024]{1,0:T(8,128)S(1)}, u32[]{:S(2)}, u32[]{:S(2)}) %collective-permute-start.1) | collective-permute-done | bytes 262176 | tf_op jit(solution)/shard_map/ppermute | solution.py:53
  113.7 2.5 collective-permute-start.2
  116.2 3.3 %collective-permute-done.2 = f32[64,1024]{1,0:T(8,128)S(1)} collective-permute-done((f32[64,1024]{1,0:T(8,128)S(1)}, f32[64,1024]{1,0:T(8,128)S(1)}, u32[]{:S(2)}, u32[]{:S(2)}) %collective-permute-start.2) | collective-permute-done | bytes 262176 | tf_op jit(solution)/shard_map/ppermute | solution.py:53
  119.5 2.5 collective-permute-start.3
  122.0 3.3 %collective-permute-done.3 = f32[64,1024]{1,0:T(8,128)S(1)} collective-permute-done((f32[64,1024]{1,0:T(8,128)S(1)}, f32[64,1024]{1,0:T(8,128)S(1)}, u32[]{:S(2)}, u32[]{:S(2)}) %collective-permute-start.3) | collective-permute-done | bytes 262176 | tf_op jit(solution)/shard_map/ppermute | solution.py:53
  125.3 2.5 collective-permute-start.4
  127.8 3.8 %collective-permute-done.4 = f32[64,1024]{1,0:T(8,128)S(1)} collective-permute-done((f32[64,1024]{1,0:T(8,128)S(1)}, f32[64,1024]{1,0:T(8,128)S(1)}, u32[]{:S(2)}, u32[]{:S(2)}) %collective-permute-start.4) | collective-permute-done | bytes 262176 | tf_op jit(solution)/shard_map/ppermute | solution.py:53
  131.6 2.0 collective-permute-start.5
  133.6 5.6 %collective-permute-done.5 = f32[64,1024]{1,0:T(8,128)S(1)} collective-permute-done((f32[64,1024]{1,0:T(8,128)S(1)}, f32[64,1024]{1,0:T(8,128)S(1)}, u32[]{:S(2)}, u32[]{:S(2)}) %collective-permute-start.5) | collective-permute-done | bytes 262176 | tf_op jit(solution)/shard_map/ppermute | solution.py:53
  139.4 7.4 %collective-permute-done.6 = f32[64,1024]{1,0:T(8,128)S(1)} collective-permute-done((f32[64,1024]{1,0:T(8,128)S(1)}, f32[64,1024]{1,0:T(8,128)S(1)}, u32[]{:S(2)}, u32[]{:S(2)}) %collective-permute-start.6) | collective-permute-done | bytes 262176 | tf_op jit(solution)/shard_map/ppermute | solution.py:53
  147.2 1.6 multiply_reduce_fusion.1
  148.8 1.6 multiply_reduce_fusion
  151.7 1.2 copy.56
  153.0 54.0 %psum.7 = f32[]{:T(128)} all-reduce(f32[]{:T(128)S(6)} %add.41), channel_id=1, replica_groups=mesh['fs'=8,'tp'=4] {'fs','tp'}, use_global_device_ids=true, to_apply=%region_4.5 | all-reduce | flops 1 | bytes 8 | tf_op jit(solution)/shard_map/psum | solution.py:61
  208.5 1.2 copy.55
  210.6 1.0 copy.58
  211.6 1.0 copy.60
  212.6 1.0 copy.57
  214.6 26.7 %all-gather.5.cloned.1.call-done = bf16[2048,512]{0,1:T(8,128)(2,1)} async-done(((bf16[256,512]{0,1:T(8,128)(2,1)}), bf16[2048,512]{0,1:T(8,128)(2,1)}) %all-gather.5.cloned.1.call-update) | async-done | bytes 2097168 | tf_op jit(solution)/shard_map/all_gather | solution.py:69
  241.3 3.9 %copy.62 = bf16[2048,512]{1,0:T(8,128)(2,1)} copy(bf16[2048,512]{0,1:T(8,128)(2,1)} %all-gather.5.cloned.1.call-done) | data formatting | bytes 4194304
  245.2 27.8 %all-gather.3.cloned.1.call-done = bf16[2048,512]{0,1:T(8,128)(2,1)} async-done(((bf16[256,512]{0,1:T(8,128)(2,1)}), bf16[2048,512]{0,1:T(8,128)(2,1)}) %all-gather.3.cloned.1.call-update) | async-done | bytes 2097168 | tf_op jit(solution)/shard_map/all_gather | solution.py:68
  273.0 3.9 %copy.61 = bf16[2048,512]{1,0:T(8,128)(2,1)} copy(bf16[2048,512]{0,1:T(8,128)(2,1)} %all-gather.3.cloned.1.call-done) | data formatting | bytes 4194304
  (42 shorter events, 3.5 us)
Async XLA Ops:
  7.2 60.7 %copy-start = (bf16[256,512]{1,0:T(8,128)(2,1)S(1)}, bf16[256,512]{1,0:T(8,128)(2,1)}, u32[]{:S(2)}) copy-start(bf16[256,512]{1,0:T(8,128)(2,1)} %param.16) | copy-start | bytes 786436
  7.2 59.5 %reduce-scatter.5.cloned.1.call-start = ((), (), s32[]{:S(2)}) async-start(), calls=%async_computation.2 | async-start | bytes 4718592 | tf_op jit(solution)/shard_map/reduce_scatter | solution.py:27
  16.6 50.0 %copy-start.1 = (bf16[256,512]{1,0:T(8,128)(2,1)S(1)}, bf16[256,512]{1,0:T(8,128)(2,1)}, u32[]{:S(2)}) copy-start(bf16[256,512]{1,0:T(8,128)(2,1)} %param.17) | copy-start | bytes 786436
  16.6 84.9 %reduce-scatter.7.cloned.1.call-start = ((), (), s32[]{:S(2)}) async-start(), calls=%async_computation.5 | async-start | bytes 2359296 | tf_op jit(solution)/shard_map/reduce_scatter | solution.py:39
  69.3 32.3 %copy-start.2 = (f32[64,512]{1,0:T(8,128)S(1)}, f32[64,512]{1,0:T(8,128)}, u32[]{:S(2)}) copy-start(f32[64,512]{1,0:T(8,128)} %param.20) | copy-start | bytes 393220
  69.4 32.2 %copy-start.3 = (f32[64,512]{1,0:T(8,128)S(1)}, f32[64,512]{1,0:T(8,128)}, u32[]{:S(2)}) copy-start(f32[64,512]{1,0:T(8,128)} %param.18) | copy-start | bytes 393220
  69.4 32.2 %copy-start.4 = (f32[64,512]{1,0:T(8,128)S(1)}, f32[64,512]{1,0:T(8,128)}, u32[]{:S(2)}) copy-start(f32[64,512]{1,0:T(8,128)} %param.21) | copy-start | bytes 393220
  69.4 32.2 %copy-start.5 = (f32[64,512]{1,0:T(8,128)S(1)}, f32[64,512]{1,0:T(8,128)}, u32[]{:S(2)}) copy-start(f32[64,512]{1,0:T(8,128)} %param.19) | copy-start | bytes 393220
  71.2 170.1 %all-gather.5.cloned.1.call-start = ((), (), s32[]{:S(2)}) async-start(), calls=%async_computation.4 | async-start | bytes 2359296 | tf_op jit(solution)/shard_map/all_gather | solution.py:69
  103.4 4.4 %collective-permute-start = (f32[64,1024]{1,0:T(8,128)S(1)}, f32[64,1024]{1,0:T(8,128)S(1)}, u32[]{:S(2)}, u32[]{:S(2)}) collective-permute-start(f32[64,1024]{1,0:T(8,128)S(1)} %pad_maximum_fusion.1), channel_id=1, source_target_pairs={{0,4},{4,8},{8,12},{12,16},{16,20},{20,24},{24,28},{28,0},{1,5},{5... | collective-permute-start | bytes 786440 | tf_op jit(solution)/shard_map/ppermute | solution.py:53
  107.9 5.8 %collective-permute-start.1 = (f32[64,1024]{1,0:T(8,128)S(1)}, f32[64,1024]{1,0:T(8,128)S(1)}, u32[]{:S(2)}, u32[]{:S(2)}) collective-permute-start(f32[64,1024]{1,0:T(8,128)S(1)} %collective-permute-done), channel_id=1, source_target_pairs={{0,4},{4,8},{8,12},{12,16},{16,20},{20,24},{24,28},{28,0},{1,5},{5... | collective-permute-start | bytes 786440 | tf_op jit(solution)/shard_map/ppermute | solution.py:53
  113.7 5.8 %collective-permute-start.2 = (f32[64,1024]{1,0:T(8,128)S(1)}, f32[64,1024]{1,0:T(8,128)S(1)}, u32[]{:S(2)}, u32[]{:S(2)}) collective-permute-start(f32[64,1024]{1,0:T(8,128)S(1)} %collective-permute-done.1), channel_id=1, source_target_pairs={{0,4},{4,8},{8,12},{12,16},{16,20},{20,24},{24,28},{28,0},{1,5},{5... | collective-permute-start | bytes 786440 | tf_op jit(solution)/shard_map/ppermute | solution.py:53
  119.5 5.8 %collective-permute-start.3 = (f32[64,1024]{1,0:T(8,128)S(1)}, f32[64,1024]{1,0:T(8,128)S(1)}, u32[]{:S(2)}, u32[]{:S(2)}) collective-permute-start(f32[64,1024]{1,0:T(8,128)S(1)} %collective-permute-done.2), channel_id=1, source_target_pairs={{0,4},{4,8},{8,12},{12,16},{16,20},{20,24},{24,28},{28,0},{1,5},{5... | collective-permute-start | bytes 786440 | tf_op jit(solution)/shard_map/ppermute | solution.py:53
  125.3 6.3 %collective-permute-start.4 = (f32[64,1024]{1,0:T(8,128)S(1)}, f32[64,1024]{1,0:T(8,128)S(1)}, u32[]{:S(2)}, u32[]{:S(2)}) collective-permute-start(f32[64,1024]{1,0:T(8,128)S(1)} %collective-permute-done.3), channel_id=1, source_target_pairs={{0,4},{4,8},{8,12},{12,16},{16,20},{20,24},{24,28},{28,0},{1,5},{5... | collective-permute-start | bytes 786440 | tf_op jit(solution)/shard_map/ppermute | solution.py:53
  131.6 7.6 %collective-permute-start.5 = (f32[64,1024]{1,0:T(8,128)S(1)}, f32[64,1024]{1,0:T(8,128)S(1)}, u32[]{:S(2)}, u32[]{:S(2)}) collective-permute-start(f32[64,1024]{1,0:T(8,128)S(1)} %collective-permute-done.4), channel_id=1, source_target_pairs={{0,4},{4,8},{8,12},{12,16},{16,20},{20,24},{24,28},{28,0},{1,5},{5... | collective-permute-start | bytes 786440 | tf_op jit(solution)/shard_map/ppermute | solution.py:53
  139.2 7.6 %collective-permute-start.6 = (f32[64,1024]{1,0:T(8,128)S(1)}, f32[64,1024]{1,0:T(8,128)S(1)}, u32[]{:S(2)}, u32[]{:S(2)}) collective-permute-start(f32[64,1024]{1,0:T(8,128)S(1)} %collective-permute-done.5), channel_id=1, source_target_pairs={{0,4},{4,8},{8,12},{12,16},{16,20},{20,24},{24,28},{28,0},{1,5},{5... | collective-permute-start | bytes 786440 | tf_op jit(solution)/shard_map/ppermute | solution.py:53
  208.5 64.5 %all-gather.3.cloned.1.call-start = ((), (), s32[]{:S(2)}) async-start(), calls=%async_computation.3 | async-start | bytes 2359296 | tf_op jit(solution)/shard_map/all_gather | solution.py:68
Sparse Core Ops, SparseCore 0:
  16.8 49.8 reduce-scatter.4
  71.3 30.1 reduce-scatter.6
  208.6 32.6 all-gather.4
  243.3 29.6 all-gather.2
